TPU v7x, 32 devices: a whole 2x2x4 slice. The times are simulated.
32 devices in a mesh: tp: 8 (over z, y), dp: 4 (over x, core).
Axes of the slice: x: 2, y: 2, z: 4, core: 2. Of those that a mesh axis runs over, the one named last changes fastest.
Arguments:
- tokens: bfloat16 [192, 8448], P('dp', 'tp'), may hold values from -6 to 6
- gains: float32 [2, 8448], replicated, may hold values from 0.1 to 1.9
- w_input: bfloat16 [2, 8448, 12288], P(None, 'dp', 'tp'), may hold values from -0.0625 to 0.0625
- w_gating: bfloat16 [2, 8448, 12288], P(None, 'dp', 'tp'), may hold values from -0.0625 to 0.0625
- w_output: bfloat16 [2, 12288, 8448], P(None, 'tp'), may hold values from -0.21875 to 0.21875
- decay_rate: float32 [2, 768, 64], P(None, 'tp'), may hold values from 0.05 to 2
- frequency: float32 [2, 768, 64], P(None, 'tp'), may hold values from -3 to 3
- log_step: float32 [2, 768], P(None, 'tp'), may hold values from -2.3 to 0
- in_real: float32 [2, 768, 64, 16], P(None, 'tp'), may hold values from -1 to 1
- in_imag: float32 [2, 768, 64, 16], P(None, 'tp'), may hold values from -1 to 1
- readout_real_matrix: float32 [2, 768, 16, 64], P(None, 'tp'), may hold values from -0.5 to 0.5
- readout_imag_matrix: float32 [2, 768, 16, 64], P(None, 'tp'), may hold values from -0.5 to 0.5
- skip_gain: float32 [2, 12288], P(None, 'tp'), may hold values from -4 to 4
- state_real: float32 [2, 192, 768, 64], P(None, 'dp', 'tp'), may hold values from -6 to 6
- state_imag: float32 [2, 192, 768, 64], P(None, 'dp', 'tp'), may hold values from -6 to 6
Outputs:
- mixed: bfloat16 [192, 8448], P('dp', 'tp')
- next_real: float32 [2, 192, 768, 64], P(None, 'dp', 'tp')
- next_imag: float32 [2, 192, 768, 64], P(None, 'dp', 'tp')
All inputs are finite; a program needn't handle non-finite values.
Results may differ from a plain program's by a relative error of at most 0.008.
Values may be sent and summed in bfloat16 or wider, within the bound.
A program may use at most 256 MiB of HBM per device.

v0:
```python
import jax
import jax.numpy as jnp
from jax import lax
from jax.sharding import PartitionSpec as P

GS = 16
LAYERS = 2
PRECISION_LEVEL = lax.Precision.HIGHEST


def collect(shard):
    return lax.all_gather(shard, "tp", axis=1, tiled=True)


def spread(partial_value):
    return lax.psum_scatter(partial_value, "tp", scatter_dimension=1, tiled=True)


def on_device(
    tokens,
    gains,
    w_input,
    w_gating,
    w_output,
    decay_rate,
    frequency,
    log_step,
    in_real,
    in_imag,
    readout_real_matrix,
    readout_imag_matrix,
    skip_gain,
    state_real,
    state_imag,
):
    width = tokens.shape[1]
    offset = lax.axis_index("tp") * width
    batch = tokens.shape[0]
    groups = decay_rate.shape[1]
    shard = tokens
    whole = collect(shard)
    outs_re = []
    outs_im = []
    for layer_params in range(LAYERS):
        xf = whole.astype(jnp.float32)
        meansq = jnp.mean(xf * xf, axis=1, keepdims=True)
        inverse = lax.rsqrt(meansq + 1e-06)
        scaled = (xf * gains[layer_params][None, :]).astype(jnp.bfloat16)
        drive = jnp.dot(
            scaled,
            lax.all_gather(w_input[layer_params], "dp", axis=0, tiled=True),
            preferred_element_type=jnp.float32,
        )
        gate = jnp.dot(
            scaled,
            lax.all_gather(w_gating[layer_params], "dp", axis=0, tiled=True),
            preferred_element_type=jnp.float32,
        )
        drive = drive * inverse
        gate = gate * inverse
        step = jnp.exp(log_step[layer_params])[:, None]
        lam_re = -decay_rate[layer_params]
        lam_im = frequency[layer_params]
        magnitude = jnp.exp(lam_re * step)
        angle = lam_im * step
        abar_re = magnitude * jnp.cos(angle)
        abar_im = magnitude * jnp.sin(angle)
        denom = lam_re * lam_re + lam_im * lam_im
        num_re = abar_re - 1.0
        zoh_re = (num_re * lam_re + abar_im * lam_im) / denom
        zoh_im = (abar_im * lam_re - num_re * lam_im) / denom
        bbar_re = (
            zoh_re[..., None] * in_real[layer_params] - zoh_im[..., None] * in_imag[layer_params]
        )
        bbar_im = (
            zoh_re[..., None] * in_imag[layer_params] + zoh_im[..., None] * in_real[layer_params]
        )
        grouped = drive.reshape(batch, groups, GS)
        push_re = jnp.einsum("bgc,gpc->bgp", grouped, bbar_re, precision=PRECISION_LEVEL)
        push_im = jnp.einsum("bgc,gpc->bgp", grouped, bbar_im, precision=PRECISION_LEVEL)
        old_re = state_real[layer_params]
        old_im = state_imag[layer_params]
        updated_real = abar_re[None] * old_re - abar_im[None] * old_im + push_re
        updated_imag = abar_re[None] * old_im + abar_im[None] * old_re + push_im
        readout_output = jnp.einsum(
            "zju,jiu->zji",
            updated_real,
            readout_real_matrix[layer_params],
            precision=PRECISION_LEVEL,
        ) - jnp.einsum(
            "zju,jiu->zji",
            updated_imag,
            readout_imag_matrix[layer_params],
            precision=PRECISION_LEVEL,
        )
        readout_output = (
            readout_output + skip_gain[layer_params].reshape(groups, GS)[None] * grouped
        )
        gated = (
            jax.nn.gelu(readout_output.reshape(batch, groups * GS)) * jax.nn.sigmoid(gate)
        ).astype(jnp.bfloat16)
        partial_value = jnp.dot(gated, w_output[layer_params], preferred_element_type=jnp.float32)
        outs_re.append(updated_real)
        outs_im.append(updated_imag)
        if layer_params + 1 < LAYERS:
            summed = lax.psum(partial_value, "tp")
            whole = (xf + summed).astype(jnp.bfloat16)
        else:
            own = lax.dynamic_slice_in_dim(whole, offset, width, 1)
            shard = (own.astype(jnp.float32) + spread(partial_value)).astype(jnp.bfloat16)
    return (shard, jnp.stack(outs_re, axis=0), jnp.stack(outs_im, axis=0))


def solution(mesh):
    placed = (
        P("dp", "tp"),
        P(),
        P(None, "dp", "tp"),
        P(None, "dp", "tp"),
        P(None, "tp", None),
        P(None, "tp", None),
        P(None, "tp", None),
        P(None, "tp"),
        P(None, "tp", None, None),
        P(None, "tp", None, None),
        P(None, "tp", None, None),
        P(None, "tp", None, None),
        P(None, "tp"),
        P(None, "dp", "tp", None),
        P(None, "dp", "tp", None),
    )
    return jax.shard_map(
        on_device,
        mesh=mesh,
        in_specs=placed,
        out_specs=(P("dp", "tp"), P(None, "dp", "tp", None), P(None, "dp", "tp", None)),
        check_vma=False,
    )
```

profile of v0, /device:TPU:0, one launch (start us, length us, event | category | flops | bytes accessed | tf_op | source)
XLA Modules:
  0.0 894.9 jit_solution(3569177894118164036)
XLA Ops:
  7.2 10.3 %fusion.143 = (bf16[1,2112,1536]{2,1,0:T(8,128)(2,1)}, bf16[1,2112,1536]{2,1,0:T(8,128)(2,1)}) fusion(bf16[2,2112,1536]{2,1,0:T(8,128)(2,1)} %param.17), kind=kLoop, calls=%fused_computation.162 | loop fusion | bytes 25952256 | tf_op jit(solution)/shard_map/slice | solution.py:51
  17.6 10.7 %fusion.144 = (bf16[1,2112,1536]{2,1,0:T(8,128)(2,1)}, bf16[1,2112,1536]{2,1,0:T(8,128)(2,1)}) fusion(bf16[2,2112,1536]{2,1,0:T(8,128)(2,1)} %param.18), kind=kLoop, calls=%fused_computation.163 | loop fusion | bytes 25952256 | tf_op jit(solution)/shard_map/slice | solution.py:56
  28.4 0.6 copy-done.40
  29.2 0.3 fusion.125
  29.5 0.5 copy-done.24
  29.9 0.6 copy-done.25
  30.6 1.3 fusion.92
  31.9 1.3 copy.82
  33.2 34.4 %all-gather.4 = bf16[8,1056,48]{1,2,0:T(8,128)(2,1)S(1)} all-gather(bf16[1,1056,48]{1,2,0:T(8,128)(2,1)S(1)} %bitcast.329), channel_id=1, replica_groups=mesh['tp'=8,'dp'=4] {'tp'}, dimensions={0}, use_global_device_ids=true | all-gather | bytes 912384 | tf_op jit(solution)/shard_map/all_gather | solution.py:12
  67.8 0.5 reshape.330
  68.3 0.9 multiply_bitcast_fusion.1
  69.2 0.7 copy.77
  69.9 0.7 copy.79
  70.6 3.5 fusion.145
  74.1 1.9 copy.109
  76.0 3.5 fusion.146
  79.5 1.9 copy.110
  81.4 2.2 fusion.148
  83.6 1.2 copy.111
  84.8 1.3 copy.84
  86.1 2.1 fusion.147
  88.2 1.2 copy.112
  89.4 0.6 slice_reduce_fusion.2
  90.0 0.7 mul.494
  90.7 0.7 slice_reduce_fusion
  91.7 87.8 %all-gather.10.cloned.1.call-done = bf16[1,8448,1536]{2,1,0:T(8,128)(2,1)} async-done(((bf16[1,2112,1536]{2,1,0:T(8,128)(2,1)}), bf16[1,8448,1536]{2,1,0:T(8,128)(2,1)}) %all-gather.10.cloned.1.call-update) | async-done | bytes 25952272 | tf_op jit(solution)/shard_map/all_gather | solution.py:51
  179.5 11.5 %fusion.21 = f32[48,1536]{1,0:T(8,128)S(1)} fusion(bf16[1,8448,1536]{2,1,0:T(8,128)(2,1)} %all-gather.10.cloned.1.call-done, f32[8448,48]{0,1:T(8,128)S(1)} %reshape.330, f32[8448]{0:T(1024)S(1)} %get-tuple-element.13, f32[48]{0:T(128)S(1)} %add_rsqrt_fusion.1), kind=kOutput, calls=%fused_computation.33 | convolution fusion | flops 1246593024 | bytes 27903168 | tf_op jit(solution)/shard_map/dot_general | solution.py:49
  191.1 0.3 copy.81
  191.4 6.7 bitcast_add_fusion.3
  198.2 3.8 fusion.86
  202.0 3.9 bitcast_add_fusion.2
  206.0 3.8 fusion.81
  209.8 0.2 copy.90
  210.0 130.3 %all-gather.12.cloned.1.call-done = bf16[1,8448,1536]{2,1,0:T(8,128)(2,1)} async-done(((bf16[1,2112,1536]{2,1,0:T(8,128)(2,1)}), bf16[1,8448,1536]{2,1,0:T(8,128)(2,1)}) %all-gather.12.cloned.1.call-update) | async-done | bytes 25952272 | tf_op jit(solution)/shard_map/all_gather | solution.py:56
  340.3 20.3 %fusion.6 = f32[48,8448]{1,0:T(8,128)} fusion(bf16[2,1536,8448]{2,1,0:T(8,128)(2,1)} %param.19, bf16[1,8448,1536]{2,1,0:T(8,128)(2,1)} %all-gather.12.cloned.1.call-done, f32[48,1536]{1,0:T(8,128)S(1)} %copy.90, f32[8448,48]{0,1:T(8,128)S(1)} %reshape.330, f32[8448]{0:T(1024)S(1)} %get-tuple-element.13, f32[48]{0:T(128)S(1)} %add_rsqrt_fusion.1), kind=kOutput, calls=%fused_computation.6 | convolution fusion | flops 2493259776 | bytes 55477440 | tf_op jit(solution)/shard_map/dot_general | solution.py:102
  360.6 0.5 all-gather.14.cloned.1.call-update
  361.2 0.5 all-gather.16.cloned.1.call-update
  361.8 2.3 copy.98
  364.2 0.7 copy.93
  364.9 1.9 copy.113
  366.8 3.0 copy.114
  369.9 1.3 copy.96
  371.2 1.2 copy.115
  372.4 1.2 copy.116
  373.7 0.7 mul.541
  374.3 76.9 %all-reduce.2.cloned.1.call-done = f32[48,8448]{1,0:T(8,128)} async-done(((f32[48,8448]{1,0:T(8,128)}), f32[48,8448]{1,0:T(8,128)}) %all-reduce.2.cloned.1.call-update) | async-done | bytes 1622032 | tf_op jit(solution)/shard_map/psum | solution.py:106
  451.2 1.7 fusion.74
  452.9 158.2 %all-gather.14.cloned.1.call-done = bf16[1,8448,1536]{2,1,0:T(8,128)(2,1)} async-done(((bf16[1,2112,1536]{2,1,0:T(8,128)(2,1)}), bf16[1,8448,1536]{2,1,0:T(8,128)(2,1)}) %all-gather.14.cloned.1.call-update) | async-done | bytes 25952272 | tf_op jit(solution)/shard_map/all_gather | solution.py:51
  611.1 12.0 %fusion.42 = f32[48,1536]{1,0:T(8,128)S(1)} fusion(bf16[1,8448,1536]{2,1,0:T(8,128)(2,1)} %all-gather.14.cloned.1.call-done, bf16[48,8448]{1,0:T(8,128)(2,1)S(1)} %get-tuple-element.17, f32[8448]{0:T(1024)S(1)} %copy-done.31, f32[48]{0:T(128)S(1)} %add_rsqrt_fusion), kind=kOutput, calls=%fused_computation.40 | convolution fusion | flops 1246998528 | bytes 27092160 | tf_op jit(solution)/shard_map/dot_general | solution.py:49
  623.1 0.3 copy.95
  623.4 6.6 bitcast_add_fusion.1
  630.0 3.8 fusion.83
  633.8 4.0 bitcast_add_fusion
  637.9 4.0 fusion.79
  642.2 129.5 %all-gather.16.cloned.1.call-done = bf16[1,8448,1536]{2,1,0:T(8,128)(2,1)} async-done(((bf16[1,2112,1536]{2,1,0:T(8,128)(2,1)}), bf16[1,8448,1536]{2,1,0:T(8,128)(2,1)}) %all-gather.16.cloned.1.call-update) | async-done | bytes 25952272 | tf_op jit(solution)/shard_map/all_gather | solution.py:56
  771.7 22.6 %fusion.14 = f32[8448,48]{1,0:T(8,128)} fusion(bf16[2,1536,8448]{2,1,0:T(8,128)(2,1)} %param.19, bf16[1,8448,1536]{2,1,0:T(8,128)(2,1)} %all-gather.16.cloned.1.call-done, bf16[48,8448]{1,0:T(8,128)(2,1)S(1)} %copy-done.12, f32[8448]{0:T(1024)S(1)} %copy-done.31, f32[48,1536]{1,0:T(8,128)S(1)} %copy.104, f32[48]{0:T(128)S(1)} %add_rsqrt_fusion), kind=kOutput, calls=%fused_computation.14 | convolution fusion | flops 2493665280 | bytes 54666432
  794.3 1.6 copy-done.3
  796.0 4.1 pad_maximum_fusion.1
  800.1 5.7 copy.106
  805.8 4.1 pad_maximum_fusion
  809.9 5.8 copy.105
  815.7 69.0 %reduce-scatter.4.cloned.1.call-done = f32[1056,48]{1,0:T(8,128)} async-done(((f32[8448,48]{1,0:T(8,128)}), f32[1056,48]{1,0:T(8,128)}) %reduce-scatter.4.cloned.1.call-update) | async-done | bytes 202768
  884.7 1.3 copy.108
  886.0 1.7 add_convert_fusion
  (95 shorter events, 1.5 us)
Async XLA Ops:
  7.2 172.4 %all-gather.10.cloned.1.call-start = ((), (), s32[]{:S(2)}) async-start(), calls=%async_computation.2 | async-start | bytes 32440320 | tf_op jit(solution)/shard_map/all_gather | solution.py:51
  17.5 322.8 %all-gather.12.cloned.1.call-start = ((), (), s32[]{:S(2)}) async-start(), calls=%async_computation.3 | async-start | bytes 32440320 | tf_op jit(solution)/shard_map/all_gather | solution.py:56
  28.3 0.7 copy-start.40
  28.3 0.9 copy-start.29
  28.3 0.9 copy-start.30
  28.3 1.7 copy-start.24
  28.3 2.3 copy-start.25
  28.3 422.9 %all-reduce.2.cloned.1.call-start = ((), (), s32[]{:S(2)}) async-start(), calls=%async_computation.1 | async-start | bytes 3244032 | tf_op jit(solution)/shard_map/psum | solution.py:106
  30.6 2.6 copy-start.36
  81.4 3.4 copy-start.21
  84.8 4.7 copy-start.39
  84.8 6.0 copy-start.37
  179.5 11.8 %copy-start.13 = (f32[96,64,16]{1,2,0:T(8,128)S(1)}, f32[96,64,16]{1,2,0:T(8,128)}, u32[]{:S(2)}) copy-start(f32[96,64,16]{1,2,0:T(8,128)} %copy.82) | copy-start | bytes 1179652
  191.3 6.8 copy-start.19
  191.4 10.6 %copy-start.9 = (f32[1,48,96,64]{3,1,2,0:T(8,128)S(1)}, f32[1,48,96,64]{3,1,2,0:T(8,128)}, u32[]{:S(2)}) copy-start(f32[1,48,96,64]{3,1,2,0:T(8,128)} %copy.110) | copy-start | bytes 3538948
  198.1 7.8 copy-start
  198.1 3.8 copy-start.7
  198.1 3.8 copy-start.15
  198.2 3.8 copy-start.26
  198.2 3.8 copy-start.27
  202.0 4.0 copy-start.17
  202.0 4.0 copy-start.33
  206.0 3.8 copy-start.2
  360.6 250.5 %all-gather.14.cloned.1.call-start = ((), (), s32[]{:S(2)}) async-start(), calls=%async_computation.4 | async-start | bytes 32440320 | tf_op jit(solution)/shard_map/all_gather | solution.py:51
  361.2 410.5 %all-gather.16.cloned.1.call-start = ((), (), s32[]{:S(2)}) async-start(), calls=%async_computation.5 | async-start | bytes 32440320 | tf_op jit(solution)/shard_map/all_gather | solution.py:56
  361.2 2.9 copy-start.35
  361.2 3.0 copy-start.34
  361.2 3.7 copy-start.10
  361.7 523.0 %reduce-scatter.4.cloned.1.call-start = ((), (), s32[]{:S(2)}) async-start(), calls=%async_computation.6 | async-start | bytes 4866048
  366.8 3.1 copy-start.20
  366.8 4.4 copy-start.22
  366.8 5.6 copy-start.23
  369.9 3.8 copy-start.38
  373.6 237.5 %copy-start.31 = (f32[8448]{0:T(1024)S(1)}, f32[8448]{0:T(1024)}, u32[]{:S(2)}) copy-start(f32[8448]{0:T(1024)} %get-tuple-element.12) | copy-start | bytes 101380
  452.9 158.2 %copy-start.11 = (bf16[48,8448]{1,0:T(8,128)(2,1)}, bf16[48,8448]{1,0:T(8,128)(2,1)S(1)}, u32[]{:S(2)}) copy-start(bf16[48,8448]{1,0:T(8,128)(2,1)S(1)} %get-tuple-element.17) | copy-start | bytes 2433028
  611.1 12.2 %copy-start.6 = (f32[1,48,96,64]{3,1,2,0:T(8,128)S(1)}, f32[1,48,96,64]{3,1,2,0:T(8,128)}, u32[]{:S(2)}) copy-start(f32[1,48,96,64]{3,1,2,0:T(8,128)} %copy.113) | copy-start | bytes 3538948
  623.4 6.6 copy-start.18
  630.0 7.9 copy-start.4
  630.0 3.8 copy-start.8
  630.0 3.8 copy-start.14
  630.0 3.8 copy-start.28
  633.8 4.0 copy-start.16
  633.8 4.0 copy-start.32
  637.9 4.1 copy-start.5
  637.9 133.8 %copy-start.12 = (bf16[48,8448]{1,0:T(8,128)(2,1)S(1)}, bf16[48,8448]{1,0:T(8,128)(2,1)}, u32[]{:S(2)}) copy-start(bf16[48,8448]{1,0:T(8,128)(2,1)} %copy-done.11) | copy-start | bytes 2433028
  794.3 1.7 copy-start.3
  800.1 5.7 copy-start.1
Sparse Core Ops, SparseCore 0:
  17.6 161.8 all-gather.9
  181.1 159.1 all-gather.11
  360.7 90.4 all-reduce.1
  452.6 158.4 all-gather.13
  612.5 159.1 all-gather.15
  794.4 90.2 reduce-scatter.3
where the time goes:
time: 902 us; the launch traced here: 895 us
  waiting for transfers between devices  653 us (72%)
  matrix products  103 us (11%)
  local copies, waits for them, and re-layouts  75.2 us (8%)
  blocking collectives  34.4 us (4%)
  between operations  15 us (2%)
  other arithmetic  14.3 us (2%)
    all_gather x2, waiting for transfers between devices, on_device(): lax.all_gather(w_gating[layer_params], 'dp', axis=0, tiled=True)  260 us
    all_gather x2, waiting for transfers between devices, on_device(): lax.all_gather(w_input[layer_params], 'dp', axis=0, tiled=True)  246 us
    psum x1, waiting for transfers between devices, on_device(): summed = lax.psum(partial_value, 'tp')  76.9 us
    unnamed x7, waiting for transfers between devices  70.1 us
    all_gather x1, blocking collectives, collect(): return lax.all_gather(shard, 'tp', axis=1, tiled=True)  34.4 us
    unnamed x93, local copies, waits for them, and re-layouts  30.1 us
    dot_general x2, matrix products, on_device(): jnp.dot(scaled, lax.all_gather(w_input[layer_params], 'dp', axis=0, tiled...  23.5 us
    unnamed x1, matrix products  22.6 us
  transfers between devices with their start and end apart: 6, of which 6 were waited for; matrix products, arithmetic and copies ran while one was open for 15% of the time, Pallas kernels for 0%

commit v1 on v0

--- a/solution.py
+++ b/solution.py
@@ -103,7 +103,7 @@
         outs_re.append(updated_real)
         outs_im.append(updated_imag)
         if layer_params + 1 < LAYERS:
-            summed = lax.psum(partial_value, "tp")
+            summed = jnp.sum(lax.all_gather(partial_value, "tp"), axis=0)
             whole = (xf + summed).astype(jnp.bfloat16)
         else:
             own = lax.dynamic_slice_in_dim(whole, offset, width, 1)

time: 902 us -> 991 us (1.099)
  waiting for transfers between devices: 653 us -> 738 us
    all_gather x0 -> x1, waiting for transfers between devices: none -> 168 us  [on_device(): summed = jnp.sum(lax.all_gather(partial_value, 'tp'), axis=0)]
    psum x1 -> x0, waiting for transfers between devices: 76.9 us -> none  [on_device(): summed = lax.psum(partial_value, 'tp')]
    unnamed x93 -> x87, local copies, waits for them, and re-layouts: 30.1 us -> 30.2 us
  transfers between devices with their start and end apart: 6 -> 6, of which waited for: 6 -> 6; matrix products, arithmetic and copies ran while one was open for 15% -> 14% of each run, Pallas kernels for 0% -> 0%
where the time goes in v1:
time: 991 us; the launch traced here: 984 us
  waiting for transfers between devices  738 us (74%)
  matrix products  104 us (10%)
  local copies, waits for them, and re-layouts  74.1 us (7%)
  blocking collectives  34.4 us (3%)
  other arithmetic  19.2 us (2%)
  between operations  14.8 us (1%)
    all_gather x2, waiting for transfers between devices, on_device(): lax.all_gather(w_gating[layer_params], 'dp', axis=0, tiled=True)  259 us
    all_gather x2, waiting for transfers between devices, on_device(): lax.all_gather(w_input[layer_params], 'dp', axis=0, tiled=True)  240 us
    all_gather x1, waiting for transfers between devices, on_device(): summed = jnp.sum(lax.all_gather(partial_value, 'tp'), axis=0)  168 us
    unnamed x7, waiting for transfers between devices  70.1 us
    all_gather x1, blocking collectives, collect(): return lax.all_gather(shard, 'tp', axis=1, tiled=True)  34.4 us
    unnamed x87, local copies, waits for them, and re-layouts  30.2 us
    dot_general x2, matrix products, on_device(): jnp.dot(scaled, lax.all_gather(w_input[layer_params], 'dp', axis=0, tiled...  24.1 us
    unnamed x1, matrix products  22.6 us
  transfers between devices with their start and end apart: 6, of which 6 were waited for; matrix products, arithmetic and copies ran while one was open for 14% of the time, Pallas kernels for 0%

profile of v1, /device:TPU:0, one launch (start us, length us, event | category | flops | bytes accessed | tf_op | source)
XLA Modules:
  0.0 984.0 jit_solution(9917616298487372663)
XLA Ops:
  7.2 10.3 %fusion.143 = (bf16[1,2112,1536]{2,1,0:T(8,128)(2,1)}, bf16[1,2112,1536]{2,1,0:T(8,128)(2,1)}) fusion(bf16[2,2112,1536]{2,1,0:T(8,128)(2,1)} %param.17), kind=kLoop, calls=%fused_computation.162 | loop fusion | bytes 25952256 | tf_op jit(solution)/shard_map/slice | solution.py:51
  17.6 10.7 %fusion.144 = (bf16[1,2112,1536]{2,1,0:T(8,128)(2,1)}, bf16[1,2112,1536]{2,1,0:T(8,128)(2,1)}) fusion(bf16[2,2112,1536]{2,1,0:T(8,128)(2,1)} %param.18), kind=kLoop, calls=%fused_computation.163 | loop fusion | bytes 25952256 | tf_op jit(solution)/shard_map/slice | solution.py:56
  28.4 0.6 copy-done.37
  29.2 0.3 fusion.125
  29.5 0.5 copy-done.23
  29.9 0.6 copy-done.24
  30.6 1.2 fusion.92
  31.8 1.3 copy.112
  33.1 34.4 %all-gather.5 = bf16[8,1056,48]{1,2,0:T(8,128)(2,1)S(1)} all-gather(bf16[1,1056,48]{1,2,0:T(8,128)(2,1)S(1)} %bitcast.331), channel_id=1, replica_groups=mesh['tp'=8,'dp'=4] {'tp'}, dimensions={0}, use_global_device_ids=true | all-gather | bytes 912384 | tf_op jit(solution)/shard_map/all_gather | solution.py:12
  67.7 0.5 reshape.331
  68.3 0.9 multiply_bitcast_fusion.1
  69.1 0.7 copy.107
  69.8 0.7 copy.109
  70.5 3.4 fusion.145
  74.0 1.9 copy.139
  75.9 3.5 fusion.146
  79.4 1.9 copy.140
  81.3 2.2 fusion.148
  83.5 1.3 copy.141
  84.8 1.3 copy.114
  86.1 2.1 fusion.147
  88.2 1.2 copy.142
  89.5 0.7 mul.494
  90.2 0.7 slice_reduce_fusion
  91.1 88.4 %all-gather.12.cloned.1.call-done = bf16[1,8448,1536]{2,1,0:T(8,128)(2,1)} async-done(((bf16[1,2112,1536]{2,1,0:T(8,128)(2,1)}), bf16[1,8448,1536]{2,1,0:T(8,128)(2,1)}) %all-gather.12.cloned.1.call-update) | async-done | bytes 25952272 | tf_op jit(solution)/shard_map/all_gather | solution.py:51
  179.5 11.5 %fusion.21 = f32[48,1536]{1,0:T(8,128)S(1)} fusion(bf16[1,8448,1536]{2,1,0:T(8,128)(2,1)} %all-gather.12.cloned.1.call-done, f32[8448,48]{0,1:T(8,128)S(1)} %reshape.331, f32[8448]{0:T(1024)S(1)} %get-tuple-element.16, f32[48]{0:T(128)S(1)} %add_rsqrt_fusion.1), kind=kOutput, calls=%fused_computation.33 | convolution fusion | flops 1246593024 | bytes 27903168 | tf_op jit(solution)/shard_map/dot_general | solution.py:49
  191.1 0.3 copy.111
  191.4 6.7 bitcast_add_fusion.3
  198.2 3.8 fusion.86
  202.0 3.9 bitcast_add_fusion.2
  206.0 3.8 fusion.81
  209.8 0.2 copy.120
  210.0 130.3 %all-gather.14.cloned.1.call-done = bf16[1,8448,1536]{2,1,0:T(8,128)(2,1)} async-done(((bf16[1,2112,1536]{2,1,0:T(8,128)(2,1)}), bf16[1,8448,1536]{2,1,0:T(8,128)(2,1)}) %all-gather.14.cloned.1.call-update) | async-done | bytes 25952272 | tf_op jit(solution)/shard_map/all_gather | solution.py:56
  340.3 20.3 %fusion.6 = f32[48,8448]{1,0:T(8,128)} fusion(bf16[2,1536,8448]{2,1,0:T(8,128)(2,1)} %param.19, bf16[1,8448,1536]{2,1,0:T(8,128)(2,1)} %all-gather.14.cloned.1.call-done, f32[48,1536]{1,0:T(8,128)S(1)} %copy.120, f32[8448,48]{0,1:T(8,128)S(1)} %reshape.331, f32[8448]{0:T(1024)S(1)} %get-tuple-element.16, f32[48]{0:T(128)S(1)} %add_rsqrt_fusion.1), kind=kOutput, calls=%fused_computation.6 | convolution fusion | flops 2493259776 | bytes 55477440 | tf_op jit(solution)/shard_map/dot_general | solution.py:102
  360.6 0.5 all-gather.18.cloned.1.call-update
  361.2 0.5 all-gather.20.cloned.1.call-update
  361.8 2.3 copy.128
  364.3 1.9 copy.143
  366.2 3.0 copy.144
  369.3 1.3 copy.126
  370.6 1.2 copy.145
  371.8 1.2 copy.146
  373.1 0.7 mul.541
  373.8 167.9 %all-gather.16.cloned.1.call-done = f32[384,8448]{1,0:T(8,128)} async-done(((f32[48,8448]{1,0:T(8,128)}), f32[384,8448]{1,0:T(8,128)}) %all-gather.16.cloned.1.call-update) | async-done | bytes 12976144 | tf_op jit(solution)/shard_map/all_gather | solution.py:106
  541.6 5.5 reduce_sum.28
  547.1 1.2 fusion.74
  548.3 152.1 %all-gather.18.cloned.1.call-done = bf16[1,8448,1536]{2,1,0:T(8,128)(2,1)} async-done(((bf16[1,2112,1536]{2,1,0:T(8,128)(2,1)}), bf16[1,8448,1536]{2,1,0:T(8,128)(2,1)}) %all-gather.18.cloned.1.call-update) | async-done | bytes 25952272 | tf_op jit(solution)/shard_map/all_gather | solution.py:51
  700.4 12.6 %fusion.42 = f32[48,1536]{1,0:T(8,128)S(1)} fusion(bf16[1,8448,1536]{2,1,0:T(8,128)(2,1)} %all-gather.18.cloned.1.call-done, bf16[48,8448]{1,0:T(8,128)(2,1)} %get-tuple-element.20, f32[8448]{0:T(1024)} %get-tuple-element.15, f32[48]{0:T(128)S(1)} %add_rsqrt_fusion), kind=kOutput, calls=%fused_computation.40 | convolution fusion | flops 1246998528 | bytes 27092160 | tf_op jit(solution)/shard_map/dot_general | solution.py:49
  713.0 0.3 copy.125
  713.3 6.8 bitcast_add_fusion.1
  720.1 3.8 fusion.83
  723.9 4.0 bitcast_add_fusion
  727.9 3.9 fusion.79
  731.9 0.2 copy.134
  732.1 128.9 %all-gather.20.cloned.1.call-done = bf16[1,8448,1536]{2,1,0:T(8,128)(2,1)} async-done(((bf16[1,2112,1536]{2,1,0:T(8,128)(2,1)}), bf16[1,8448,1536]{2,1,0:T(8,128)(2,1)}) %all-gather.20.cloned.1.call-update) | async-done | bytes 25952272 | tf_op jit(solution)/shard_map/all_gather | solution.py:56
  861.0 22.6 %fusion.14 = f32[8448,48]{1,0:T(8,128)} fusion(bf16[2,1536,8448]{2,1,0:T(8,128)(2,1)} %param.19, bf16[1,8448,1536]{2,1,0:T(8,128)(2,1)} %all-gather.20.cloned.1.call-done, bf16[48,8448]{1,0:T(8,128)(2,1)S(1)} %copy-done.11, f32[8448]{0:T(1024)S(1)} %copy-done.29, f32[48,1536]{1,0:T(8,128)S(1)} %copy.134, f32[48]{0:T(128)S(1)} %add_rsqrt_fusion), kind=kOutput, calls=%fused_computation.14 | convolution fusion | flops 2493665280 | bytes 54666432
  883.6 1.6 copy-done.3
  885.3 4.1 pad_maximum_fusion.1
  889.4 5.7 copy.136
  895.1 4.1 pad_maximum_fusion
  899.2 5.8 copy.135
  905.0 69.0 %reduce-scatter.4.cloned.1.call-done = f32[1056,48]{1,0:T(8,128)} async-done(((f32[8448,48]{1,0:T(8,128)}), f32[1056,48]{1,0:T(8,128)}) %reduce-scatter.4.cloned.1.call-update) | async-done | bytes 202768
  974.0 1.3 copy.138
  975.3 1.7 add_convert_fusion
  (90 shorter events, 1.3 us)
Async XLA Ops:
  7.2 172.4 %all-gather.12.cloned.1.call-start = ((), (), s32[]{:S(2)}) async-start(), calls=%async_computation.1 | async-start | bytes 32440320 | tf_op jit(solution)/shard_map/all_gather | solution.py:51
  17.5 322.7 %all-gather.14.cloned.1.call-start = ((), (), s32[]{:S(2)}) async-start(), calls=%async_computation.2 | async-start | bytes 32440320 | tf_op jit(solution)/shard_map/all_gather | solution.py:56
  28.3 0.7 copy-start.37
  28.3 0.9 copy-start.27
  28.3 0.9 copy-start.28
  28.3 1.7 copy-start.23
  28.3 2.3 copy-start.24
  28.3 513.3 %all-gather.16.cloned.1.call-start = ((), (), s32[]{:S(2)}) async-start(), calls=%async_computation.3 | async-start | bytes 14598144 | tf_op jit(solution)/shard_map/all_gather | solution.py:106
  30.6 2.6 copy-start.34
  81.3 3.5 copy-start.20
  84.8 4.7 copy-start.36
  84.8 5.4 copy-start.35
  179.5 11.8 %copy-start.12 = (f32[96,64,16]{1,2,0:T(8,128)S(1)}, f32[96,64,16]{1,2,0:T(8,128)}, u32[]{:S(2)}) copy-start(f32[96,64,16]{1,2,0:T(8,128)} %copy.112) | copy-start | bytes 1179652
  191.3 6.8 copy-start.18
  191.3 10.6 %copy-start.9 = (f32[1,48,96,64]{3,1,2,0:T(8,128)S(1)}, f32[1,48,96,64]{3,1,2,0:T(8,128)}, u32[]{:S(2)}) copy-start(f32[1,48,96,64]{3,1,2,0:T(8,128)} %copy.140) | copy-start | bytes 3538948
  198.1 7.8 copy-start
  198.1 3.8 copy-start.8
  198.1 3.8 copy-start.14
  198.2 3.8 copy-start.25
  198.2 3.8 copy-start.26
  202.0 4.0 copy-start.17
  202.0 4.0 copy-start.31
  206.0 3.8 copy-start.2
  360.6 339.8 %all-gather.18.cloned.1.call-start = ((), (), s32[]{:S(2)}) async-start(), calls=%async_computation.4 | async-start | bytes 32440320 | tf_op jit(solution)/shard_map/all_gather | solution.py:51
  361.2 499.8 %all-gather.20.cloned.1.call-start = ((), (), s32[]{:S(2)}) async-start(), calls=%async_computation.5 | async-start | bytes 32440320 | tf_op jit(solution)/shard_map/all_gather | solution.py:56
  361.2 2.9 copy-start.33
  361.2 3.0 copy-start.32
  361.2 3.1 copy-start.10
  361.7 612.3 %reduce-scatter.4.cloned.1.call-start = ((), (), s32[]{:S(2)}) async-start(), calls=%async_computation.6 | async-start | bytes 4866048
  366.2 3.1 copy-start.19
  366.2 4.4 copy-start.21
  366.2 5.6 copy-start.22
  700.4 12.8 %copy-start.6 = (f32[1,48,96,64]{3,1,2,0:T(8,128)S(1)}, f32[1,48,96,64]{3,1,2,0:T(8,128)}, u32[]{:S(2)}) copy-start(f32[1,48,96,64]{3,1,2,0:T(8,128)} %copy.143) | copy-start | bytes 3538948
  713.2 6.8 copy-start.16
  720.0 7.8 copy-start.4
  720.0 3.8 copy-start.7
  720.1 3.8 copy-start.13
  723.8 4.0 copy-start.15
  723.8 4.0 copy-start.30
  727.9 4.0 copy-start.5
  727.9 133.1 %copy-start.11 = (bf16[48,8448]{1,0:T(8,128)(2,1)S(1)}, bf16[48,8448]{1,0:T(8,128)(2,1)}, u32[]{:S(2)}) copy-start(bf16[48,8448]{1,0:T(8,128)(2,1)} %get-tuple-element.20) | copy-start | bytes 2433028
  727.9 133.1 %copy-start.29 = (f32[8448]{0:T(1024)S(1)}, f32[8448]{0:T(1024)}, u32[]{:S(2)}) copy-start(f32[8448]{0:T(1024)} %get-tuple-element.15) | copy-start | bytes 101380
  883.6 1.7 copy-start.3
  889.4 5.7 copy-start.1
Sparse Core Ops, SparseCore 0:
  17.6 161.8 all-gather.11
  181.1 159.1 all-gather.13
  360.7 180.8 all-gather.15
  543.1 157.2 all-gather.17
  701.8 159.1 all-gather.19
  883.7 90.2 reduce-scatter.3
